TPU v7x, 32 devices: a whole 2x2x4 slice. The times are simulated.
32 devices in a mesh: fs: 8 (over z, y), tp: 4 (over x, core).
Axes of the slice: x: 2, y: 2, z: 4, core: 2. Of those that a mesh axis runs over, the one named last changes fastest.
Arguments:
- stream: bfloat16 [4096, 1024], P(('fs', 'tp')), may hold values from -3 to 3
- mixer_out: bfloat16 [4096, 1024], P(('fs', 'tp')), may hold values from -6 to 6
- ffn_gains: float32 [4, 1024], replicated, may hold values from 0.5 to 1.5
- mixer_gain: float32 [1024], replicated, may hold values from 0.25 to 0.6
- gate_first: bfloat16 [1024, 2816], P('fs', 'tp'), may hold values from -0.1875 to 0.1875
- up_first: bfloat16 [1024, 2816], P('fs', 'tp'), may hold values from -0.1875 to 0.1875
- down_first: bfloat16 [2816, 1024], P('tp', 'fs'), may hold values from -0.109375 to 0.109375
- gate_second: bfloat16 [1024, 2816], P('fs', 'tp'), may hold values from -0.1875 to 0.1875
- up_second: bfloat16 [1024, 2816], P('fs', 'tp'), may hold values from -0.1875 to 0.1875
- down_second: bfloat16 [2816, 1024], P('tp', 'fs'), may hold values from -0.109375 to 0.109375
Outputs:
- layer_out: bfloat16 [4096, 1024], P(('fs', 'tp'))
All inputs are finite; a program needn't handle non-finite values.
Results may differ from a plain program's by a relative error of at most 0.02.
Values may be sent and summed in bfloat16 or wider, within the bound.
A program may use at most 64 MiB of HBM per device.

v0:
```python
import jax
import jax.numpy as jnp
from jax import lax
from jax.sharding import PartitionSpec as P

epsilon = 1e-06
half_weight = 0.5


def over_all(section, axis, dim, apply):
    everything = lax.all_gather(section, axis, axis=dim, tiled=True)
    return apply(everything, jnp.int32(0))


def summed_rows(portion, rows, axis):
    count = rows * lax.axis_size(axis)
    sent = portion(jnp.int32(0), count).astype(jnp.bfloat16)
    return lax.psum_scatter(sent, axis, scatter_dimension=0, tiled=True).astype(jnp.float32)


def rms_rows(values, gain_row):
    widened = values.astype(jnp.float32)
    inverse_rms = lax.rsqrt(jnp.mean(widened * widened, axis=-1, keepdims=True) + epsilon)
    return (widened * inverse_rms * gain_row.astype(jnp.float32)).astype(jnp.bfloat16)


def add_branch(rows, normed_branch, factor):
    return (rows.astype(jnp.float32) + factor * normed_branch.astype(jnp.float32)).astype(
        jnp.bfloat16
    )


def collect_weights(gate_local, up_local, down_local):
    gate_full, up_full = (
        lax.all_gather(gate_local, "fs", axis=0, tiled=True),
        lax.all_gather(up_local, "fs", axis=0, tiled=True),
    )
    down_full = lax.all_gather(down_local, "fs", axis=1, tiled=True)
    return (gate_full, up_full, down_full)


def half_step(rows, gain_pre, gain_post, weight_set):
    gate_full, up_full, down_full = weight_set
    normed = rms_rows(rows, gain_pre)

    def activate(tokens_part, first_row):
        gate_sum = jnp.dot(tokens_part, gate_full, preferred_element_type=jnp.float32)
        up_sum = jnp.dot(tokens_part, up_full, preferred_element_type=jnp.float32)
        return (jax.nn.silu(gate_sum) * up_sum).astype(jnp.bfloat16)

    hidden = over_all(normed, "tp", 0, activate)

    def project(first_row, row_count):
        row_block = lax.dynamic_slice_in_dim(hidden, first_row, row_count, 0)
        return jnp.dot(row_block, down_full, preferred_element_type=jnp.float32)

    branch = summed_rows(project, normed.shape[0], "tp").astype(jnp.bfloat16)
    return add_branch(rows, rms_rows(branch, gain_post), half_weight)


def on_device(
    stream,
    mixer_out,
    ffn_gains,
    mixer_gain,
    gate_first,
    up_first,
    down_first,
    gate_second,
    up_second,
    down_second,
):
    first_set = collect_weights(gate_first, up_first, down_first)
    after_first = half_step(stream, ffn_gains[0], ffn_gains[1], first_set)
    mixed_in = add_branch(after_first, rms_rows(mixer_out, mixer_gain), 1.0)
    second_set = collect_weights(gate_second, up_second, down_second)
    return half_step(mixed_in, ffn_gains[2], ffn_gains[3], second_set)


def solution(mesh):
    in_specs = (
        P(("fs", "tp"), None),
        P(("fs", "tp"), None),
        P(),
        P(),
        P("fs", "tp"),
        P("fs", "tp"),
        P("tp", "fs"),
        P("fs", "tp"),
        P("fs", "tp"),
        P("tp", "fs"),
    )
    out_specs = P(("fs", "tp"), None)
    return jax.shard_map(
        on_device, mesh=mesh, in_specs=in_specs, out_specs=out_specs, check_vma=False
    )
```

profile of v0, /device:TPU:0, one launch (start us, length us, event | category | flops | bytes accessed | tf_op | source)
XLA Modules:
  0.0 376.5 jit_solution(1594553680892777717)
XLA Ops:
  6.5 0.9 fusion.23
  7.4 1.1 fusion.13
  8.5 1.8 fusion.15
  10.4 0.7 all-gather.11.cloned.1.call-update
  12.4 17.5 %all-gather.9.cloned.1.call-done = bf16[512,1024]{1,0:T(8,128)(2,1)} async-done(((bf16[128,1024]{1,0:T(8,128)(2,1)}), bf16[512,1024]{1,0:T(8,128)(2,1)}) %all-gather.9.cloned.1.call-update) | async-done | bytes 1048592 | tf_op jit(solution)/shard_map/all_gather | solution.py:11
  29.9 45.1 %all-gather.11.cloned.1.call-done = bf16[1024,704]{0,1:T(8,128)(2,1)} async-done(((bf16[128,704]{0,1:T(8,128)(2,1)}), bf16[1024,704]{0,1:T(8,128)(2,1)}) %all-gather.11.cloned.1.call-update) | async-done | bytes 1441808 | tf_op jit(solution)/shard_map/all_gather | solution.py:35
  75.0 2.6 fusion.24
  77.6 40.6 %all-gather.13.cloned.1.call-done = bf16[1024,704]{0,1:T(8,128)(2,1)} async-done(((bf16[128,704]{0,1:T(8,128)(2,1)}), bf16[1024,704]{0,1:T(8,128)(2,1)}) %all-gather.13.cloned.1.call-update) | async-done | bytes 1441808 | tf_op jit(solution)/shard_map/all_gather | solution.py:36
  118.2 43.1 %all-gather.15.cloned.1.call-done = bf16[704,1024]{1,0:T(8,128)(2,1)} async-done(((bf16[704,128]{1,0:T(8,128)(2,1)}), bf16[704,1024]{1,0:T(8,128)(2,1)}) %all-gather.15.cloned.1.call-update) | async-done | bytes 1441808 | tf_op jit(solution)/shard_map/all_gather | solution.py:38
  161.3 4.7 %convolution_convert_fusion.1 = bf16[512,1024]{1,0:T(8,128)(2,1)} fusion(bf16[704,1024]{1,0:T(8,128)(2,1)} %all-gather.15.cloned.1.call-done, bf16[512,1024]{1,0:T(8,128)(2,1)S(1)} %copy-done.3, bf16[1024,704]{0,1:T(8,128)(2,1)} %all-gather.13.cloned.1.call-done, f32[512,704]{0,1:T(8,128)S(1)} %fusion.24), kind=kOutput, calls=%fused_computation.1 | convolution fusion | flops 1479081984 | bytes 6422528 | tf_op jit(solution)/shard_map/dot_general | solution.py:55
  166.8 22.3 %reduce-scatter.3.cloned.1.call-done = bf16[128,1024]{1,0:T(8,128)(2,1)} async-done(((bf16[512,1024]{1,0:T(8,128)(2,1)}), bf16[128,1024]{1,0:T(8,128)(2,1)}) %reduce-scatter.3.cloned.1.call-update) | async-done | bytes 262160 | tf_op jit(solution)/shard_map/reduce_scatter | solution.py:18
  189.2 1.1 fusion.4
  190.3 1.3 fusion.17
  191.6 0.8 fusion.19
  192.5 0.7 all-gather.21.cloned.1.call-update
  194.0 40.0 %all-gather.19.cloned.1.call-done = bf16[1024,704]{0,1:T(8,128)(2,1)} async-done(((bf16[128,704]{0,1:T(8,128)(2,1)}), bf16[1024,704]{0,1:T(8,128)(2,1)}) %all-gather.19.cloned.1.call-update) | async-done | bytes 1441808 | tf_op jit(solution)/shard_map/all_gather | solution.py:35
  234.1 16.5 %all-gather.17.cloned.1.call-done = bf16[512,1024]{1,0:T(8,128)(2,1)} async-done(((bf16[128,1024]{1,0:T(8,128)(2,1)}), bf16[512,1024]{1,0:T(8,128)(2,1)}) %all-gather.17.cloned.1.call-update) | async-done | bytes 1048592 | tf_op jit(solution)/shard_map/all_gather | solution.py:11
  250.5 2.7 fusion.25
  253.2 42.3 %all-gather.21.cloned.1.call-done = bf16[1024,704]{0,1:T(8,128)(2,1)} async-done(((bf16[128,704]{0,1:T(8,128)(2,1)}), bf16[1024,704]{0,1:T(8,128)(2,1)}) %all-gather.21.cloned.1.call-update) | async-done | bytes 1441808 | tf_op jit(solution)/shard_map/all_gather | solution.py:36
  295.6 43.2 %all-gather.23.cloned.1.call-done = bf16[704,1024]{1,0:T(8,128)(2,1)} async-done(((bf16[704,128]{1,0:T(8,128)(2,1)}), bf16[704,1024]{1,0:T(8,128)(2,1)}) %all-gather.23.cloned.1.call-update) | async-done | bytes 1441808 | tf_op jit(solution)/shard_map/all_gather | solution.py:38
  338.8 4.7 %convolution_convert_fusion = bf16[512,1024]{1,0:T(8,128)(2,1)} fusion(bf16[704,1024]{1,0:T(8,128)(2,1)} %all-gather.23.cloned.1.call-done, bf16[512,1024]{1,0:T(8,128)(2,1)S(1)} %copy-done.4, bf16[1024,704]{0,1:T(8,128)(2,1)} %all-gather.21.cloned.1.call-done, f32[512,704]{0,1:T(8,128)S(1)} %fusion.25), kind=kOutput, calls=%fused_computation | convolution fusion | flops 1479081984 | bytes 6422528 | tf_op jit(solution)/shard_map/dot_general | solution.py:55
  343.6 23.1 %reduce-scatter.5.cloned.1.call-done = bf16[128,1024]{1,0:T(8,128)(2,1)} async-done(((bf16[512,1024]{1,0:T(8,128)(2,1)}), bf16[128,1024]{1,0:T(8,128)(2,1)}) %reduce-scatter.5.cloned.1.call-update) | async-done | bytes 262160 | tf_op jit(solution)/shard_map/reduce_scatter | solution.py:18
  366.7 1.1 fusion.10
  367.8 1.8 fusion.20
  (34 shorter events, 3.0 us)
Async XLA Ops:
  6.5 23.4 %all-gather.9.cloned.1.call-start = ((), (), s32[]{:S(2)}) async-start(), calls=%async_computation.2 | async-start | bytes 1310720 | tf_op jit(solution)/shard_map/all_gather | solution.py:11
  10.3 64.6 %all-gather.11.cloned.1.call-start = ((), (), s32[]{:S(2)}) async-start(), calls=%async_computation.3 | async-start | bytes 1622016 | tf_op jit(solution)/shard_map/all_gather | solution.py:35
  11.1 107.1 %all-gather.13.cloned.1.call-start = ((), (), s32[]{:S(2)}) async-start(), calls=%async_computation.4 | async-start | bytes 1622016 | tf_op jit(solution)/shard_map/all_gather | solution.py:36
  11.8 149.5 %all-gather.15.cloned.1.call-start = ((), (), s32[]{:S(2)}) async-start(), calls=%async_computation.5 | async-start | bytes 1622016 | tf_op jit(solution)/shard_map/all_gather | solution.py:38
  12.4 176.8 %reduce-scatter.3.cloned.1.call-start = ((), (), s32[]{:S(2)}) async-start(), calls=%async_computation.6 | async-start | bytes 1310720 | tf_op jit(solution)/shard_map/reduce_scatter | solution.py:18
  29.9 131.4 %copy-start.3 = (bf16[512,1024]{1,0:T(8,128)(2,1)S(1)}, bf16[512,1024]{1,0:T(8,128)(2,1)}, u32[]{:S(2)}) copy-start(bf16[512,1024]{1,0:T(8,128)(2,1)} %all-gather.9.cloned.1.call-done) | copy-start | bytes 3145732
  77.6 89.1 %copy-start.1 = (bf16[128,1024]{1,0:T(8,128)(2,1)S(1)}, bf16[128,1024]{1,0:T(8,128)(2,1)}, u32[]{:S(2)}) copy-start(bf16[128,1024]{1,0:T(8,128)(2,1)} %param.11) | copy-start | bytes 786436
  166.0 24.2 %copy-start = (bf16[128,1024]{1,0:T(8,128)(2,1)S(1)}, bf16[128,1024]{1,0:T(8,128)(2,1)}, u32[]{:S(2)}) copy-start(bf16[128,1024]{1,0:T(8,128)(2,1)} %param.10) | copy-start | bytes 786436
  166.0 24.3 %copy-start.2 = (f32[1024]{0:T(1024)S(1)}, f32[1024]{0:T(1024)}, u32[]{:S(2)}) copy-start(f32[1024]{0:T(1024)} %param.13) | copy-start | bytes 12292
  166.0 68.0 %all-gather.19.cloned.1.call-start = ((), (), s32[]{:S(2)}) async-start(), calls=%async_computation.8 | async-start | bytes 1622016 | tf_op jit(solution)/shard_map/all_gather | solution.py:35
  166.6 83.9 %all-gather.17.cloned.1.call-start = ((), (), s32[]{:S(2)}) async-start(), calls=%async_computation.7 | async-start | bytes 1310720 | tf_op jit(solution)/shard_map/all_gather | solution.py:11
  192.5 103.1 %all-gather.21.cloned.1.call-start = ((), (), s32[]{:S(2)}) async-start(), calls=%async_computation.9 | async-start | bytes 1622016 | tf_op jit(solution)/shard_map/all_gather | solution.py:36
  193.2 145.6 %all-gather.23.cloned.1.call-start = ((), (), s32[]{:S(2)}) async-start(), calls=%async_computation.10 | async-start | bytes 1622016 | tf_op jit(solution)/shard_map/all_gather | solution.py:38
  194.0 172.7 %reduce-scatter.5.cloned.1.call-start = ((), (), s32[]{:S(2)}) async-start(), calls=%async_computation.11 | async-start | bytes 1310720 | tf_op jit(solution)/shard_map/reduce_scatter | solution.py:18
  250.5 88.3 %copy-start.4 = (bf16[512,1024]{1,0:T(8,128)(2,1)S(1)}, bf16[512,1024]{1,0:T(8,128)(2,1)}, u32[]{:S(2)}) copy-start(bf16[512,1024]{1,0:T(8,128)(2,1)} %all-gather.17.cloned.1.call-done) | copy-start | bytes 3145732
Sparse Core Ops, SparseCore 0:
  10.4 19.4 all-gather.8
  31.9 42.9 all-gather.10
  77.0 41.1 all-gather.12
  120.1 41.1 all-gather.14
  166.2 22.9 reduce-scatter.2
  191.1 42.9 all-gather.18
  235.6 14.8 all-gather.16
  252.6 42.9 all-gather.20
  297.6 41.1 all-gather.22
  343.7 22.9 reduce-scatter.4
where the time goes:
time: 377 us; the launch traced here: 376 us
  waiting for transfers between devices  338 us (90%)
  matrix products  14.8 us (4%)
  between operations  13.6 us (4%)
  other arithmetic  9.24 us (2%)
    all_gather x2, waiting for transfers between devices, collect_weights(): down_full = lax.all_gather(down_local, 'fs', axis=1, tiled=True)  86.3 us
    all_gather x2, waiting for transfers between devices, collect_weights(): lax.all_gather(gate_local, 'fs', axis=0, tiled=True)  85.1 us
    all_gather x2, waiting for transfers between devices, collect_weights(): lax.all_gather(up_local, 'fs', axis=0, tiled=True)  82.9 us
    reduce_scatter x2, waiting for transfers between devices, summed_rows(): lax.psum_scatter(sent, axis, scatter_dimension=0, tiled=True)  45.5 us
    all_gather x2, waiting for transfers between devices, over_all(): everything = lax.all_gather(section, axis, axis=dim, tiled=True)  33.9 us
    dot_general x2, matrix products, project(): return jnp.dot(row_block, down_full, preferred_element_type=jnp.float32)  9.42 us
  transfers between devices with their start and end apart: 10, of which 10 were waited for; matrix products, arithmetic and copies ran while one was open for 2% of the time, Pallas kernels for 0%

commit v1 on v0

--- a/solution.py
+++ b/solution.py
@@ -35,7 +35,12 @@
         lax.all_gather(gate_local, "fs", axis=0, tiled=True),
         lax.all_gather(up_local, "fs", axis=0, tiled=True),
     )
-    down_full = lax.all_gather(down_local, "fs", axis=1, tiled=True)
+    ring = [down_local]
+    for hop in range(7):
+        ring.append(lax.ppermute(ring[-1], "fs", [(dev, (dev + 1) % 8) for dev in range(8)]))
+    down_full = jnp.roll(
+        jnp.concatenate(ring[::-1], axis=1), (lax.axis_index("fs") + 1) * ring[0].shape[1], axis=1
+    )
     return (gate_full, up_full, down_full)
 
 

time: 377 us -> 309 us (0.82)
  waiting for transfers between devices: 338 us -> 261 us
  starting transfers between devices: 0.35 us -> 4.88 us
    ppermute x0 -> x14, waiting for transfers between devices: none -> 134 us  [collect_weights(): lax.ppermute(ring[-1], 'fs', [(dev, (dev + 1) % 8) for dev in range(8)])]
    all_gather x2 -> x0, waiting for transfers between devices: 86.3 us -> none  [collect_weights(): down_full = lax.all_gather(down_local, 'fs', axis=1, tiled=True)]
    all_gather x2, waiting for transfers between devices: 85.1 us -> 0.04 us  [collect_weights(): lax.all_gather(gate_local, 'fs', axis=0, tiled=True)]
    all_gather x2, waiting for transfers between devices: 33.9 us -> 0.04 us  [over_all(): everything = lax.all_gather(section, axis, axis=dim, tiled=True)]
    ppermute x0 -> x14, starting transfers between devices: none -> 4.6 us  [collect_weights(): lax.ppermute(ring[-1], 'fs', [(dev, (dev + 1) % 8) for dev in range(8)])]
    all_gather x2, waiting for transfers between devices: 82.9 us -> 79 us  [collect_weights(): lax.all_gather(up_local, 'fs', axis=0, tiled=True)]
  transfers between devices with their start and end apart: 10 -> 22, of which waited for: 10 -> 18; matrix products, arithmetic and copies ran while one was open for 2% -> 4% of each run, Pallas kernels for 0% -> 0%
where the time goes in v1:
time: 309 us
  waiting for transfers between devices  261 us (84%)
  matrix products  17.6 us (6%)
  between operations  13.7 us (4%)
  other arithmetic  9.24 us (3%)
  starting transfers between devices  4.88 us (2%)
    ppermute x14, waiting for transfers between devices, collect_weights(): lax.ppermute(ring[-1], 'fs', [(dev, (dev + 1) % 8) for dev in range(8)])  134 us
    all_gather x2, waiting for transfers between devices, collect_weights(): lax.all_gather(up_local, 'fs', axis=0, tiled=True)  79 us
    reduce_scatter x2, waiting for transfers between devices, summed_rows(): lax.psum_scatter(sent, axis, scatter_dimension=0, tiled=True)  45.4 us
    dot_general x2, matrix products, project(): return jnp.dot(row_block, down_full, preferred_element_type=jnp.float32)  10 us
    dot_general x2, matrix products, activate(): jnp.dot(tokens_part, gate_full, preferred_element_type=jnp.float32)  7.55 us
  transfers between devices with their start and end apart: 22, of which 18 were waited for; matrix products, arithmetic and copies ran while one was open for 4% of the time, Pallas kernels for 0%

profile of v1, /device:TPU:0, one launch (start us, length us, event | category | flops | bytes accessed | tf_op | source)
XLA Modules:
  0.0 308.5 jit_solution(17904591484580359883)
XLA Ops:
  11.9 3.0 collective-permute-start
  14.9 7.6 %collective-permute-done = bf16[704,128]{1,0:T(8,128)(2,1)S(1)} collective-permute-done((bf16[704,128]{1,0:T(8,128)(2,1)S(1)}, bf16[704,128]{1,0:T(8,128)(2,1)S(1)}, u32[]{:S(2)}, u32[]{:S(2)}) %collective-permute-start) | collective-permute-done | bytes 180256 | tf_op jit(solution)/shard_map/ppermute | solution.py:40
  22.5 8.4 %collective-permute-done.1 = bf16[704,128]{1,0:T(8,128)(2,1)S(1)} collective-permute-done((bf16[704,128]{1,0:T(8,128)(2,1)S(1)}, bf16[704,128]{1,0:T(8,128)(2,1)S(1)}, u32[]{:S(2)}, u32[]{:S(2)}) %collective-permute-start.1) | collective-permute-done | bytes 180256 | tf_op jit(solution)/shard_map/ppermute | solution.py:40
  30.9 8.2 %collective-permute-done.2 = bf16[704,128]{1,0:T(8,128)(2,1)S(1)} collective-permute-done((bf16[704,128]{1,0:T(8,128)(2,1)S(1)}, bf16[704,128]{1,0:T(8,128)(2,1)S(1)}, u32[]{:S(2)}, u32[]{:S(2)}) %collective-permute-start.2) | collective-permute-done | bytes 180256 | tf_op jit(solution)/shard_map/ppermute | solution.py:40
  39.1 10.7 %collective-permute-done.3 = bf16[704,128]{1,0:T(8,128)(2,1)S(1)} collective-permute-done((bf16[704,128]{1,0:T(8,128)(2,1)S(1)}, bf16[704,128]{1,0:T(8,128)(2,1)S(1)}, u32[]{:S(2)}, u32[]{:S(2)}) %collective-permute-start.3) | collective-permute-done | bytes 180256 | tf_op jit(solution)/shard_map/ppermute | solution.py:40
  49.9 8.3 %collective-permute-done.4 = bf16[704,128]{1,0:T(8,128)(2,1)S(1)} collective-permute-done((bf16[704,128]{1,0:T(8,128)(2,1)S(1)}, bf16[704,128]{1,0:T(8,128)(2,1)S(1)}, u32[]{:S(2)}, u32[]{:S(2)}) %collective-permute-start.4) | collective-permute-done | bytes 180256 | tf_op jit(solution)/shard_map/ppermute | solution.py:40
  58.2 11.0 %collective-permute-done.5 = bf16[704,128]{1,0:T(8,128)(2,1)S(1)} collective-permute-done((bf16[704,128]{1,0:T(8,128)(2,1)S(1)}, bf16[704,128]{1,0:T(8,128)(2,1)S(1)}, u32[]{:S(2)}, u32[]{:S(2)}) %collective-permute-start.5) | collective-permute-done | bytes 180256 | tf_op jit(solution)/shard_map/ppermute | solution.py:40
  69.2 12.1 %collective-permute-done.6 = bf16[704,128]{1,0:T(8,128)(2,1)S(1)} collective-permute-done((bf16[704,128]{1,0:T(8,128)(2,1)S(1)}, bf16[704,128]{1,0:T(8,128)(2,1)S(1)}, u32[]{:S(2)}, u32[]{:S(2)}) %collective-permute-start.6) | collective-permute-done | bytes 180256 | tf_op jit(solution)/shard_map/ppermute | solution.py:40
  81.9 3.7 %fusion.30 = f32[512,704]{0,1:T(8,128)} fusion(bf16[512,1024]{1,0:T(8,128)(2,1)} %all-gather.7.cloned.1.call-done, bf16[1024,704]{0,1:T(8,128)(2,1)} %all-gather.9.cloned.1.call-done), kind=kOutput, calls=%fused_computation.70 | convolution fusion | flops 738197504 | bytes 3932160 | tf_op jit(solution)/shard_map/dot_general | solution.py:52
  85.6 40.5 %all-gather.11.cloned.1.call-done = bf16[1024,704]{0,1:T(8,128)(2,1)} async-done(((bf16[128,704]{0,1:T(8,128)(2,1)}), bf16[1024,704]{0,1:T(8,128)(2,1)}) %all-gather.11.cloned.1.call-update) | async-done | bytes 1441808 | tf_op jit(solution)/shard_map/all_gather | solution.py:36
  126.1 5.2 %convolution_convert_fusion.1 = bf16[512,1024]{1,0:T(8,128)(2,1)} fusion(s32[]{:T(128)S(6)} %select_n.13, bf16[704,1024]{1,0:T(8,128)(2,1)S(1)} %constant_dynamic-update-slice_fusion, bf16[512,1024]{1,0:T(8,128)(2,1)} %all-gather.7.cloned.1.call-done, bf16[1024,704]{0,1:T(8,128)(2,1)} %all-gather.11.cloned.1.call-done, f32[512,704]{0,1:T(8,128)} %fusion.30), kind=kOutput, calls=%fused_computation.5 | convolution fusion | flops 1481965568 | bytes 6422532 | tf_op jit(solution)/shard_map/dot_general | solution.py:60
  132.1 22.3 %reduce-scatter.3.cloned.1.call-done = bf16[128,1024]{1,0:T(8,128)(2,1)} async-done(((bf16[512,1024]{1,0:T(8,128)(2,1)}), bf16[128,1024]{1,0:T(8,128)(2,1)}) %reduce-scatter.3.cloned.1.call-update) | async-done | bytes 262160 | tf_op jit(solution)/shard_map/reduce_scatter | solution.py:18
  160.1 7.4 %collective-permute-done.7 = bf16[704,128]{1,0:T(8,128)(2,1)S(1)} collective-permute-done((bf16[704,128]{1,0:T(8,128)(2,1)S(1)}, bf16[704,128]{1,0:T(8,128)(2,1)S(1)}, u32[]{:S(2)}, u32[]{:S(2)}) %collective-permute-start.7) | collective-permute-done | bytes 180256 | tf_op jit(solution)/shard_map/ppermute | solution.py:40
  167.5 9.9 %collective-permute-done.8 = bf16[704,128]{1,0:T(8,128)(2,1)S(1)} collective-permute-done((bf16[704,128]{1,0:T(8,128)(2,1)S(1)}, bf16[704,128]{1,0:T(8,128)(2,1)S(1)}, u32[]{:S(2)}, u32[]{:S(2)}) %collective-permute-start.8) | collective-permute-done | bytes 180256 | tf_op jit(solution)/shard_map/ppermute | solution.py:40
  177.5 8.2 %collective-permute-done.9 = bf16[704,128]{1,0:T(8,128)(2,1)S(1)} collective-permute-done((bf16[704,128]{1,0:T(8,128)(2,1)S(1)}, bf16[704,128]{1,0:T(8,128)(2,1)S(1)}, u32[]{:S(2)}, u32[]{:S(2)}) %collective-permute-start.9) | collective-permute-done | bytes 180256 | tf_op jit(solution)/shard_map/ppermute | solution.py:40
  185.7 12.5 %collective-permute-done.10 = bf16[704,128]{1,0:T(8,128)(2,1)S(1)} collective-permute-done((bf16[704,128]{1,0:T(8,128)(2,1)S(1)}, bf16[704,128]{1,0:T(8,128)(2,1)S(1)}, u32[]{:S(2)}, u32[]{:S(2)}) %collective-permute-start.10) | collective-permute-done | bytes 180256 | tf_op jit(solution)/shard_map/ppermute | solution.py:40
  198.2 12.3 %collective-permute-done.11 = bf16[704,128]{1,0:T(8,128)(2,1)S(1)} collective-permute-done((bf16[704,128]{1,0:T(8,128)(2,1)S(1)}, bf16[704,128]{1,0:T(8,128)(2,1)S(1)}, u32[]{:S(2)}, u32[]{:S(2)}) %collective-permute-start.11) | collective-permute-done | bytes 180256 | tf_op jit(solution)/shard_map/ppermute | solution.py:40
  210.5 9.3 %collective-permute-done.12 = bf16[704,128]{1,0:T(8,128)(2,1)S(1)} collective-permute-done((bf16[704,128]{1,0:T(8,128)(2,1)S(1)}, bf16[704,128]{1,0:T(8,128)(2,1)S(1)}, u32[]{:S(2)}, u32[]{:S(2)}) %collective-permute-start.12) | collective-permute-done | bytes 180256 | tf_op jit(solution)/shard_map/ppermute | solution.py:40
  219.7 8.2 %collective-permute-done.13 = bf16[704,128]{1,0:T(8,128)(2,1)S(1)} collective-permute-done((bf16[704,128]{1,0:T(8,128)(2,1)S(1)}, bf16[704,128]{1,0:T(8,128)(2,1)S(1)}, u32[]{:S(2)}, u32[]{:S(2)}) %collective-permute-start.13) | collective-permute-done | bytes 180256 | tf_op jit(solution)/shard_map/ppermute | solution.py:40
  228.5 3.8 %fusion.31 = f32[512,704]{0,1:T(8,128)} fusion(bf16[512,1024]{1,0:T(8,128)(2,1)} %all-gather.13.cloned.1.call-done, bf16[1024,704]{0,1:T(8,128)(2,1)} %all-gather.15.cloned.1.call-done), kind=kOutput, calls=%fused_computation.71 | convolution fusion | flops 738197504 | bytes 3932160 | tf_op jit(solution)/shard_map/dot_general | solution.py:52
  232.3 38.5 %all-gather.17.cloned.1.call-done = bf16[1024,704]{0,1:T(8,128)(2,1)} async-done(((bf16[128,704]{0,1:T(8,128)(2,1)}), bf16[1024,704]{0,1:T(8,128)(2,1)}) %all-gather.17.cloned.1.call-update) | async-done | bytes 1441808 | tf_op jit(solution)/shard_map/all_gather | solution.py:36
  270.8 4.9 %convolution_convert_fusion = bf16[512,1024]{1,0:T(8,128)(2,1)} fusion(s32[]{:T(128)S(6)} %select_n.13, bf16[704,1024]{1,0:T(8,128)(2,1)S(1)} %constant_dynamic-update-slice_fusion.8, bf16[512,1024]{1,0:T(8,128)(2,1)S(1)} %copy-done.5, bf16[1024,704]{0,1:T(8,128)(2,1)} %all-gather.17.cloned.1.call-done, f32[512,704]{0,1:T(8,128)} %fusion.31), kind=kOutput, calls=%fused_computation.4 | convolution fusion | flops 1481965568 | bytes 6422532 | tf_op jit(solution)/shard_map/dot_general | solution.py:60
  275.7 23.1 %reduce-scatter.5.cloned.1.call-done = bf16[128,1024]{1,0:T(8,128)(2,1)} async-done(((bf16[512,1024]{1,0:T(8,128)(2,1)}), bf16[128,1024]{1,0:T(8,128)(2,1)}) %reduce-scatter.5.cloned.1.call-update) | async-done | bytes 262160 | tf_op jit(solution)/shard_map/reduce_scatter | solution.py:18
  299.8 1.8 fusion.22
  (74 shorter events, 13.8 us)
Async XLA Ops:
  6.5 75.3 %all-gather.7.cloned.1.call-start = ((), (), s32[]{:S(2)}) async-start(), calls=%async_computation.2 | async-start | bytes 1310720 | tf_op jit(solution)/shard_map/all_gather | solution.py:11
  10.3 71.5 %all-gather.9.cloned.1.call-start = ((), (), s32[]{:S(2)}) async-start(), calls=%async_computation.3 | async-start | bytes 1622016 | tf_op jit(solution)/shard_map/all_gather | solution.py:35
  11.1 115.1 %all-gather.11.cloned.1.call-start = ((), (), s32[]{:S(2)}) async-start(), calls=%async_computation.4 | async-start | bytes 1622016 | tf_op jit(solution)/shard_map/all_gather | solution.py:36
  11.8 142.7 %reduce-scatter.3.cloned.1.call-start = ((), (), s32[]{:S(2)}) async-start(), calls=%async_computation.5 | async-start | bytes 1310720 | tf_op jit(solution)/shard_map/reduce_scatter | solution.py:18
  11.9 10.6 %collective-permute-start = (bf16[704,128]{1,0:T(8,128)(2,1)S(1)}, bf16[704,128]{1,0:T(8,128)(2,1)S(1)}, u32[]{:S(2)}, u32[]{:S(2)}) collective-permute-start(bf16[704,128]{1,0:T(8,128)(2,1)S(1)} %copy-done.2), channel_id=1, source_target_pairs={{0,4},{4,8},{8,12},{12,16},{16,20},{20,24},{24,28},{28,0},{1,5},{5... | collective-permute-start | bytes 540680 | tf_op jit(solution)/shard_map/ppermute | solution.py:40
  22.5 8.4 %collective-permute-start.1 = (bf16[704,128]{1,0:T(8,128)(2,1)S(1)}, bf16[704,128]{1,0:T(8,128)(2,1)S(1)}, u32[]{:S(2)}, u32[]{:S(2)}) collective-permute-start(bf16[704,128]{1,0:T(8,128)(2,1)S(1)} %collective-permute-done), channel_id=1, source_target_pairs={{0,4},{4,8},{8,12},{12,16},{16,20},{20,24},{24,28},{28,0},{1,5},{5... | collective-permute-start | bytes 540680 | tf_op jit(solution)/shard_map/ppermute | solution.py:40
  30.9 8.2 %collective-permute-start.2 = (bf16[704,128]{1,0:T(8,128)(2,1)S(1)}, bf16[704,128]{1,0:T(8,128)(2,1)S(1)}, u32[]{:S(2)}, u32[]{:S(2)}) collective-permute-start(bf16[704,128]{1,0:T(8,128)(2,1)S(1)} %collective-permute-done.1), channel_id=1, source_target_pairs={{0,4},{4,8},{8,12},{12,16},{16,20},{20,24},{24,28},{28,0},{1,5},{5... | collective-permute-start | bytes 540680 | tf_op jit(solution)/shard_map/ppermute | solution.py:40
  39.1 10.8 %collective-permute-start.3 = (bf16[704,128]{1,0:T(8,128)(2,1)S(1)}, bf16[704,128]{1,0:T(8,128)(2,1)S(1)}, u32[]{:S(2)}, u32[]{:S(2)}) collective-permute-start(bf16[704,128]{1,0:T(8,128)(2,1)S(1)} %collective-permute-done.2), channel_id=1, source_target_pairs={{0,4},{4,8},{8,12},{12,16},{16,20},{20,24},{24,28},{28,0},{1,5},{5... | collective-permute-start | bytes 540680 | tf_op jit(solution)/shard_map/ppermute | solution.py:40
  49.9 8.3 %collective-permute-start.4 = (bf16[704,128]{1,0:T(8,128)(2,1)S(1)}, bf16[704,128]{1,0:T(8,128)(2,1)S(1)}, u32[]{:S(2)}, u32[]{:S(2)}) collective-permute-start(bf16[704,128]{1,0:T(8,128)(2,1)S(1)} %collective-permute-done.3), channel_id=1, source_target_pairs={{0,4},{4,8},{8,12},{12,16},{16,20},{20,24},{24,28},{28,0},{1,5},{5... | collective-permute-start | bytes 540680 | tf_op jit(solution)/shard_map/ppermute | solution.py:40
  58.2 11.0 %collective-permute-start.5 = (bf16[704,128]{1,0:T(8,128)(2,1)S(1)}, bf16[704,128]{1,0:T(8,128)(2,1)S(1)}, u32[]{:S(2)}, u32[]{:S(2)}) collective-permute-start(bf16[704,128]{1,0:T(8,128)(2,1)S(1)} %collective-permute-done.4), channel_id=1, source_target_pairs={{0,4},{4,8},{8,12},{12,16},{16,20},{20,24},{24,28},{28,0},{1,5},{5... | collective-permute-start | bytes 540680 | tf_op jit(solution)/shard_map/ppermute | solution.py:40
  69.2 12.1 %collective-permute-start.6 = (bf16[704,128]{1,0:T(8,128)(2,1)S(1)}, bf16[704,128]{1,0:T(8,128)(2,1)S(1)}, u32[]{:S(2)}, u32[]{:S(2)}) collective-permute-start(bf16[704,128]{1,0:T(8,128)(2,1)S(1)} %collective-permute-done.5), channel_id=1, source_target_pairs={{0,4},{4,8},{8,12},{12,16},{16,20},{20,24},{24,28},{28,0},{1,5},{5... | collective-permute-start | bytes 540680 | tf_op jit(solution)/shard_map/ppermute | solution.py:40
  85.6 46.4 %copy-start.1 = (bf16[128,1024]{1,0:T(8,128)(2,1)S(1)}, bf16[128,1024]{1,0:T(8,128)(2,1)}, u32[]{:S(2)}) copy-start(bf16[128,1024]{1,0:T(8,128)(2,1)} %param.13) | copy-start | bytes 786436
  131.3 97.1 %all-gather.15.cloned.1.call-start = ((), (), s32[]{:S(2)}) async-start(), calls=%async_computation.7 | async-start | bytes 1622016 | tf_op jit(solution)/shard_map/all_gather | solution.py:35
  131.9 96.5 %all-gather.13.cloned.1.call-start = ((), (), s32[]{:S(2)}) async-start(), calls=%async_computation.6 | async-start | bytes 1310720 | tf_op jit(solution)/shard_map/all_gather | solution.py:11
  157.8 113.0 %all-gather.17.cloned.1.call-start = ((), (), s32[]{:S(2)}) async-start(), calls=%async_computation.8 | async-start | bytes 1622016 | tf_op jit(solution)/shard_map/all_gather | solution.py:36
  158.6 140.2 %reduce-scatter.5.cloned.1.call-start = ((), (), s32[]{:S(2)}) async-start(), calls=%async_computation.9 | async-start | bytes 1310720 | tf_op jit(solution)/shard_map/reduce_scatter | solution.py:18
  158.6 8.9 %collective-permute-start.7 = (bf16[704,128]{1,0:T(8,128)(2,1)S(1)}, bf16[704,128]{1,0:T(8,128)(2,1)S(1)}, u32[]{:S(2)}, u32[]{:S(2)}) collective-permute-start(bf16[704,128]{1,0:T(8,128)(2,1)S(1)} %copy-done.3), channel_id=1, source_target_pairs={{0,4},{4,8},{8,12},{12,16},{16,20},{20,24},{24,28},{28,0},{1,5},{5... | collective-permute-start | bytes 540680 | tf_op jit(solution)/shard_map/ppermute | solution.py:40
  167.5 9.9 %collective-permute-start.8 = (bf16[704,128]{1,0:T(8,128)(2,1)S(1)}, bf16[704,128]{1,0:T(8,128)(2,1)S(1)}, u32[]{:S(2)}, u32[]{:S(2)}) collective-permute-start(bf16[704,128]{1,0:T(8,128)(2,1)S(1)} %collective-permute-done.7), channel_id=1, source_target_pairs={{0,4},{4,8},{8,12},{12,16},{16,20},{20,24},{24,28},{28,0},{1,5},{5... | collective-permute-start | bytes 540680 | tf_op jit(solution)/shard_map/ppermute | solution.py:40
  177.5 8.2 %collective-permute-start.9 = (bf16[704,128]{1,0:T(8,128)(2,1)S(1)}, bf16[704,128]{1,0:T(8,128)(2,1)S(1)}, u32[]{:S(2)}, u32[]{:S(2)}) collective-permute-start(bf16[704,128]{1,0:T(8,128)(2,1)S(1)} %collective-permute-done.8), channel_id=1, source_target_pairs={{0,4},{4,8},{8,12},{12,16},{16,20},{20,24},{24,28},{28,0},{1,5},{5... | collective-permute-start | bytes 540680 | tf_op jit(solution)/shard_map/ppermute | solution.py:40
  185.7 12.5 %collective-permute-start.10 = (bf16[704,128]{1,0:T(8,128)(2,1)S(1)}, bf16[704,128]{1,0:T(8,128)(2,1)S(1)}, u32[]{:S(2)}, u32[]{:S(2)}) collective-permute-start(bf16[704,128]{1,0:T(8,128)(2,1)S(1)} %collective-permute-done.9), channel_id=1, source_target_pairs={{0,4},{4,8},{8,12},{12,16},{16,20},{20,24},{24,28},{28,0},{1,5},{5... | collective-permute-start | bytes 540680 | tf_op jit(solution)/shard_map/ppermute | solution.py:40
  198.2 12.3 %collective-permute-start.11 = (bf16[704,128]{1,0:T(8,128)(2,1)S(1)}, bf16[704,128]{1,0:T(8,128)(2,1)S(1)}, u32[]{:S(2)}, u32[]{:S(2)}) collective-permute-start(bf16[704,128]{1,0:T(8,128)(2,1)S(1)} %collective-permute-done.10), channel_id=1, source_target_pairs={{0,4},{4,8},{8,12},{12,16},{16,20},{20,24},{24,28},{28,0},{1,5},{5... | collective-permute-start | bytes 540680 | tf_op jit(solution)/shard_map/ppermute | solution.py:40
  210.5 9.3 %collective-permute-start.12 = (bf16[704,128]{1,0:T(8,128)(2,1)S(1)}, bf16[704,128]{1,0:T(8,128)(2,1)S(1)}, u32[]{:S(2)}, u32[]{:S(2)}) collective-permute-start(bf16[704,128]{1,0:T(8,128)(2,1)S(1)} %collective-permute-done.11), channel_id=1, source_target_pairs={{0,4},{4,8},{8,12},{12,16},{16,20},{20,24},{24,28},{28,0},{1,5},{5... | collective-permute-start | bytes 540680 | tf_op jit(solution)/shard_map/ppermute | solution.py:40
  219.7 8.2 %collective-permute-start.13 = (bf16[704,128]{1,0:T(8,128)(2,1)S(1)}, bf16[704,128]{1,0:T(8,128)(2,1)S(1)}, u32[]{:S(2)}, u32[]{:S(2)}) collective-permute-start(bf16[704,128]{1,0:T(8,128)(2,1)S(1)} %collective-permute-done.12), channel_id=1, source_target_pairs={{0,4},{4,8},{8,12},{12,16},{16,20},{20,24},{24,28},{28,0},{1,5},{5... | collective-permute-start | bytes 540680 | tf_op jit(solution)/shard_map/ppermute | solution.py:40
  228.5 42.3 %copy-start.5 = (bf16[512,1024]{1,0:T(8,128)(2,1)S(1)}, bf16[512,1024]{1,0:T(8,128)(2,1)}, u32[]{:S(2)}) copy-start(bf16[512,1024]{1,0:T(8,128)(2,1)} %all-gather.13.cloned.1.call-done) | copy-start | bytes 3145732
  (4 other events, 81.2 us)
Sparse Core Ops, SparseCore 0:
  10.5 19.4 all-gather.6
  31.9 47.9 all-gather.8
  81.9 44.1 all-gather.10
  131.5 22.9 reduce-scatter.2
  156.4 50.6 all-gather.14
  208.5 17.1 all-gather.12
  227.8 42.9 all-gather.16
  275.8 22.9 reduce-scatter.4
